TPU v7x, 32 devices: a whole 2x2x4 slice. The times are simulated.
32 devices in a mesh: sp: 4 (over z), tp: 8 (over y, x, core).
Axes of the slice: x: 2, y: 2, z: 4, core: 2. Of those that a mesh axis runs over, the one named last changes fastest.
Arguments:
- context_activations: bfloat16 [2, 1024, 4096], P(None, 'sp', 'tp'), may hold values from -6 to 6
- first_generated_activation: bfloat16 [2, 4096], replicated, may hold values from -6 to 6
- address_projection: bfloat16 [4096, 1024], P(None, 'tp'), may hold values from -0.09375 to 0.09375
- payload_projection: bfloat16 [4096, 1024], P(None, 'tp'), may hold values from -0.09375 to 0.09375
- lookup_projection: bfloat16 [4096, 1024], P(None, 'tp'), may hold values from -0.09375 to 0.09375
- exit_gating_projection: bfloat16 [4096, 1024], P(None, 'tp'), may hold values from -0.09375 to 0.09375
- writing_intensity_projection: bfloat16 [4096, 8], replicated, may hold values from -0.09375 to 0.09375
- fading_projection: bfloat16 [4096, 8], replicated, may hold values from -0.09375 to 0.09375
- channel_fading_speed: float32 [8], replicated, may hold values from 0 to 1, as said below
- extra_fading_log: float32 [2, 1024, 8], P(None, 'sp', 'tp'), may hold values from -1 to 0, as said below
- readout_normalizer_gain: float32 [128], replicated, may hold values from 0.1 to 1.9
- exit_projection: bfloat16 [1024, 4096], P('tp'), may hold values from -0.1875 to 0.1875
Outputs:
- state_cache: bfloat16 [2, 4, 8, 128, 128], P(None, 'sp', 'tp')
- step_out: bfloat16 [2, 4096], P(None, 'tp')
Inputs may be any that keep to these rules, and one draw needn't show every extreme that they name: `channel_fading_speed`: positive rates, one a head. `extra_fading_log`: zero at all but a few positions of each prompt and head, negative there.
All inputs are finite; a program needn't handle non-finite values.
Results may differ from a plain program's by a relative error of at most 0.012.
Values may be sent and summed in bfloat16 or wider, within the bound.
A program may use at most 64 MiB of HBM per device.

v0:
```python
import jax
import jax.numpy as jnp
from jax import lax
from jax.sharding import PartitionSpec as P

BLOCK = 64
norm_eps = 1e-06
highest = lax.Precision.HIGHEST


def carried_in(value, axis, combine, identity):
    devices, position = (lax.axis_size(axis), lax.axis_index(axis))
    everything = jax.tree.map(
        lambda part, kind: lax.all_gather(part.astype(kind), axis),
        value,
        (jnp.bfloat16, jnp.bfloat16),
    )
    start = jax.tree.map(
        lambda part, zero: jnp.broadcast_to(jnp.asarray(zero, part.dtype), part.shape),
        value,
        identity,
    )

    def lap(k, before):
        reached = k < position
        new = combine(
            before, jax.tree.map(lambda part, own: part[k].astype(own.dtype), everything, value)
        )
        return jax.tree.map(lambda a, b: jnp.where(reached, a, b), new, before)

    return lax.fori_loop(0, devices, lap, start)


def carried_in_2(value, axis, combine, identity):
    devices, position = (lax.axis_size(axis), lax.axis_index(axis))
    everything = lax.all_gather(value, axis)
    start = jnp.broadcast_to(jnp.asarray(identity, value.dtype), value.shape)

    def lap(k, before):
        at = devices - 1 - k
        reached = at > position
        new = combine(before, everything[at])
        return jnp.where(reached, new, before)

    return lax.fori_loop(0, devices, lap, start)


def unit_rows(values_in):
    return values_in * lax.rsqrt(jnp.sum(values_in * values_in, axis=-1, keepdims=True) + norm_eps)


def compose(left, right):
    return jnp.einsum("...ij,...jk->...ik", left, right, precision=highest)


def segment_map(keys_in, values_in, beta_gate, fading_exponent):
    blocks = keys_in.shape[0] // BLOCK
    key_blocks = keys_in.reshape(blocks, BLOCK, -1)
    value_blocks = values_in.reshape(blocks, BLOCK, -1)
    beta_blocks = beta_gate.reshape(blocks, BLOCK)
    cumul = jnp.cumsum(fading_exponent.reshape(blocks, BLOCK), axis=-1)
    causal = jnp.tril(jnp.ones((BLOCK, BLOCK), bool))
    strict = jnp.tril(jnp.ones((BLOCK, BLOCK), bool), -1)
    gaps_log = cumul[:, :, None] - cumul[:, None, :]
    within = jnp.where(causal, jnp.exp(jnp.where(causal, gaps_log, 0.0)), 0.0)
    keys_beta = key_blocks * beta_blocks[..., None]
    strict_part = jnp.where(
        strict, jnp.einsum("nid,njd->nij", keys_beta, key_blocks, precision=highest) * within, 0.0
    )
    targets = jnp.concatenate(
        [value_blocks * beta_blocks[..., None], keys_beta * jnp.exp(cumul)[..., None]], axis=-1
    )
    system = jnp.eye(BLOCK, dtype=jnp.float32) + strict_part
    solved = lax.linalg.triangular_solve(system, targets, left_side=True, lower=True)
    width_v = value_blocks.shape[-1]
    width_k = key_blocks.shape[-1]
    pseudo_values = solved[..., :width_v]
    decayed_keys = solved[..., width_v:]
    carried_values = jnp.concatenate(
        [jnp.zeros((blocks, BLOCK, width_k), jnp.float32), pseudo_values], axis=-1
    )
    trailing = key_blocks * jnp.exp(cumul[:, -1:] - cumul)[..., None]
    block_decay = jnp.exp(cumul[:, -1])

    def advance(memory, inputs):
        pseudo, decayed, trail_keys, shrink = inputs
        fresh_values = pseudo - jnp.dot(decayed, memory, precision=highest)
        memory = memory * shrink + jnp.dot(trail_keys.T, fresh_values, precision=highest)
        return (memory, None)

    start_map = jnp.concatenate(
        [jnp.eye(width_k, dtype=jnp.float32), jnp.zeros((width_k, width_v), jnp.float32)], axis=1
    )
    memory, _ = lax.scan(advance, start_map, (carried_values, decayed_keys, trailing, block_decay))
    return memory


def combine_maps(earlier, later):
    return (compose(later[0], earlier[0]), compose(later[0], earlier[1]) + later[1])


def body(
    context_activations,
    first_generated_activation,
    address_projection,
    payload_projection,
    lookup_projection,
    exit_gating_projection,
    writing_intensity_projection,
    fading_projection,
    channel_fading_speed,
    extra_fading_log,
    readout_normalizer_gain,
    exit_projection,
):
    head_size = readout_normalizer_gain.shape[0]
    current_heads = address_projection.shape[1] // head_size
    first_head = lax.axis_index("tp") * current_heads
    beta_cols = lax.dynamic_slice_in_dim(writing_intensity_projection, first_head, current_heads, 1)
    decay_cols = lax.dynamic_slice_in_dim(fading_projection, first_head, current_heads, 1)
    logit_weight = jnp.concatenate([beta_cols, decay_cols], axis=1)
    fading_speeds = lax.dynamic_slice_in_dim(channel_fading_speed, first_head, current_heads, 0)
    seq_count, length = (context_activations.shape[0], context_activations.shape[1])
    portion = lax.all_gather(context_activations, "tp", axis=2, tiled=True)
    key_sum = jnp.einsum(
        "abf,fc->abc", portion, address_projection, preferred_element_type=jnp.float32
    )
    value_sum = jnp.einsum(
        "abf,fc->abc", portion, payload_projection, preferred_element_type=jnp.float32
    )
    logit_sum = jnp.einsum("abf,fc->abc", portion, logit_weight, preferred_element_type=jnp.float32)
    shaped = (seq_count, length, current_heads, head_size)
    keys_here = unit_rows(jax.nn.silu(key_sum).reshape(shaped)).astype(jnp.bfloat16)
    values_here = jax.nn.silu(value_sum).reshape(shaped).astype(jnp.bfloat16)
    current_scores = logit_sum.astype(jnp.bfloat16)
    beta_gate = jax.nn.sigmoid(current_scores[..., :current_heads].astype(jnp.float32))
    fading_exponent = extra_fading_log - fading_speeds * jax.nn.softplus(
        current_scores[..., current_heads:].astype(jnp.float32)
    )
    maps = jax.vmap(jax.vmap(segment_map, in_axes=(1, 1, 1, 1)))(
        keys_here.astype(jnp.float32), values_here.astype(jnp.float32), beta_gate, fading_exponent
    )
    own_moves = maps[..., :head_size]
    own_offset = maps[..., head_size:]
    heads_shape = (seq_count, current_heads, head_size)
    new_keys = unit_rows(
        jax.nn.silu(
            jnp.dot(
                first_generated_activation, address_projection, preferred_element_type=jnp.float32
            )
        ).reshape(heads_shape)
    )
    new_values = jax.nn.silu(
        jnp.dot(first_generated_activation, payload_projection, preferred_element_type=jnp.float32)
    ).reshape(heads_shape)
    new_queries = unit_rows(
        jax.nn.silu(
            jnp.dot(
                first_generated_activation, lookup_projection, preferred_element_type=jnp.float32
            )
        ).reshape(heads_shape)
    )
    out_gate = jax.nn.silu(
        jnp.dot(
            first_generated_activation, exit_gating_projection, preferred_element_type=jnp.float32
        )
    ).reshape(heads_shape)
    new_logits = jnp.dot(
        first_generated_activation, logit_weight, preferred_element_type=jnp.float32
    )
    new_beta = jax.nn.sigmoid(new_logits[:, :current_heads])
    new_decay = jnp.exp(-fading_speeds * jax.nn.softplus(new_logits[:, current_heads:]))
    intersection_kq = jnp.sum(new_keys * new_queries, axis=-1, keepdims=True)
    carried_query = new_decay[..., None] * (
        new_queries - new_beta[..., None] * new_keys * intersection_kq
    )
    own_write = new_beta[..., None] * new_values * intersection_kq
    identity = jnp.broadcast_to(jnp.eye(head_size, dtype=jnp.float32), own_moves.shape)
    prefix_moves, prefix_offset = carried_in(
        (own_moves, own_offset), "sp", combine_maps, (identity, jnp.zeros_like(own_offset))
    )
    states_here = compose(own_moves, prefix_offset) + own_offset

    def chain_later(earlier, later):
        return compose(earlier, later)

    later_moves = carried_in_2(own_moves, "sp", chain_later, identity)
    lifted = jnp.einsum("shjk,shj->shk", later_moves, carried_query, precision=highest)
    term = jnp.einsum("shk,shkv->shv", lifted, own_offset, precision=highest)
    read = lax.psum(term, "sp") + own_write
    state_cache = states_here.astype(jnp.bfloat16)[:, None]
    normed = (
        read
        * lax.rsqrt(jnp.mean(read * read, axis=-1, keepdims=True) + norm_eps)
        * readout_normalizer_gain
        * out_gate
    )
    normed = normed.astype(jnp.bfloat16).reshape(seq_count, current_heads * head_size)
    partial_out = jnp.dot(normed, exit_projection, preferred_element_type=jnp.float32)
    step_out = lax.psum_scatter(partial_out, "tp", scatter_dimension=1, tiled=True).astype(
        jnp.bfloat16
    )
    return (state_cache, step_out)


def solution(mesh):
    placed = (
        P(None, "sp", "tp"),
        P(),
        P(None, "tp"),
        P(None, "tp"),
        P(None, "tp"),
        P(None, "tp"),
        P(),
        P(),
        P(),
        P(None, "sp", "tp"),
        P(),
        P("tp", None),
    )
    return jax.shard_map(
        body,
        mesh=mesh,
        in_specs=placed,
        out_specs=(P(None, "sp", "tp", None, None), P(None, "tp")),
        check_vma=False,
    )
```

profile of v0, /device:TPU:0, one launch (start us, length us, event | category | flops | bytes accessed | tf_op | source)
XLA Modules:
  0.0 188.7 jit_solution(4630512967896987474)
XLA Ops:
  7.2 0.7 all-gather.5.cloned.1.call-update
  8.1 1.3 dynamic_slice.48
  10.2 1.6 multiply_reduce_fusion.4
  11.8 1.1 multiply_reduce_fusion.3
  13.1 0.9 constant_dynamic-slice_fusion.1
  14.0 0.9 convolution_bitcast_fusion.6
  15.1 34.9 %all-gather.5.cloned.1.call-done = bf16[2,256,4096]{2,1,0:T(8,128)(2,1)} async-done(((bf16[2,256,512]{2,1,0:T(8,128)(2,1)}), bf16[2,256,4096]{2,1,0:T(8,128)(2,1)}) %all-gather.5.cloned.1.call-update) | async-done | bytes 4194320 | tf_op jit(solution)/shard_map/all_gather | solution.py:124
  50.0 3.4 %fusion.31 = bf16[2,256,2]{1,2,0:T(2,128)(2,1)S(1)} fusion(bf16[2,256,4096]{2,1,0:T(8,128)(2,1)} %all-gather.5.cloned.1.call-done, bf16[4096,1]{0,1:T(2,128)(2,1)S(1)} %get-tuple-element.365, bf16[4096,1]{0,1:T(2,128)(2,1)S(1)} %get-tuple-element.366), kind=kOutput, calls=%fused_computation.41 | convolution fusion | flops 8422400 | bytes 4212736 | tf_op jit(solution)/shard_map/abf,fc->abc/dot_general | solution.py:131
  53.3 0.7 fusion.63
  55.0 3.6 %multiply_reduce_fusion = (f32[2,256]{1,0:T(2,128)S(1)}, f32[2,256,128]{2,1,0:T(8,128)S(1)}) fusion(bf16[2,256,4096]{2,1,0:T(8,128)(2,1)} %all-gather.5.cloned.1.call-done, bf16[4096,128]{1,0:T(8,128)(2,1)S(1)} %copy-done), kind=kOutput, calls=%fused_computation.60 | convolution fusion | flops 537263616 | bytes 5507072 | tf_op jit(solution)/shard_map/abf,fc->abc/dot_general | solution.py:125
  59.1 39.3 %custom-call.3 = f32[2,1,4,1,64,64]{4,5,3,2,1,0:T(8,128)S(1)} custom-call(f32[2,1,4,1,64,64]{5,4,3,2,1,0:T(8,128)S(1)} %fusion.27), custom_call_target="InvertDiagBlocksLowerTriangular" | custom-call | tf_op jit(solution)/shard_map/vmap(vmap())/triangular_solve | solution.py:74
  98.5 3.5 %multiply_convert_fusion = bf16[2,256,128]{2,1,0:T(8,128)(2,1)S(1)} fusion(bf16[2,256,4096]{2,1,0:T(8,128)(2,1)} %all-gather.5.cloned.1.call-done, bf16[4096,128]{1,0:T(8,128)(2,1)S(1)} %copy-done.5), kind=kOutput, calls=%fused_computation.56 | convolution fusion | flops 537198592 | bytes 5373952 | tf_op jit(solution)/shard_map/abf,fc->abc/dot_general | solution.py:128
  103.1 3.0 %while.39 = (s32[]{:T(128)}, f32[2,1,128,256]{3,2,0,1:T(8,128)S(1)}, f32[4,2,1]{1,2,0:T(1,128)S(1)}, f32[4,2,1,64,128]{4,3,0,1,2:T(8,128)S(1)}, f32[4,2,1,64,256...) while((s32[]{:T(128)}, f32[2,1,128,256]{3,2,0,1:T(8,128)S(1)}, ...), condition=%wide.region_3.4_spmd, body=%wide.region_2.3_spmd.sunk | while | flops 100827136 | bytes 1312357 | solution.py:94
  106.2 16.2 %all-gather.2 = f32[8,1,128,128]{3,2,1,0:T(8,128)S(1)} all-gather(f32[2,1,128,128]{3,2,1,0:T(8,128)S(1)} %slice_bitcast_fusion.1), channel_id=4, replica_groups=mesh['sp'=4,'tp'=8] {'sp'}, dimensions={0}, use_global_device_ids=true | all-gather | bytes 655360 | tf_op jit(solution)/shard_map/all_gather | solution.py:36
  122.4 1.8 while.40
  124.7 12.1 %psum.7 = f32[2,1,128]{2,0,1:T(2,128)S(1)} all-reduce(f32[2,1,128]{2,0,1:T(2,128)S(1)} %bitcast.222), channel_id=1, replica_groups=mesh['sp'=4,'tp'=8] {'sp'}, use_global_device_ids=true, to_apply=%region_11.12 | all-reduce | flops 256 | bytes 2048 | tf_op jit(solution)/shard_map/psum | solution.py:190
  136.8 1.6 multiply_reduce_fusion.1
  138.5 3.3 %convolution_bitcast_fusion.2 = f32[4096,2]{1,0:T(8,128)} fusion(bf16[128,4096]{1,0:T(8,128)(2,1)S(1)} %copy-done.1, f32[2,1,128]{2,0,1:T(2,128)S(1)} %get-tuple-element.345, f32[128]{0:T(128)S(1)} %copy-done.4, f32[2]{0:T(128)S(1)} %add_rsqrt_fusion.1, bf16[2,4096]{1,0:T(2,128)(2,1)S(1)} %copy-done.2, bf16[4096,128]{1,0:T(8,128)(2,1)} %param.23), kind=kOutput, calls=%fused_computation.29 | convolution fusion | flops 4196352 | bytes 2147848
  141.8 14.4 %all-gather = bf16[8,1,128,128]{3,2,1,0:T(8,128)(2,1)S(1)} all-gather(bf16[2,1,128,128]{3,2,1,0:T(8,128)(2,1)S(1)} %get-tuple-element.355), channel_id=2, replica_groups=mesh['sp'=4,'tp'=8] {'sp'}, dimensions={0}, use_global_device_ids=true | all-gather | bytes 327680 | tf_op jit(solution)/shard_map/all_gather | solution.py:14
  156.2 13.8 %all-gather.1 = bf16[8,1,128,128]{3,2,1,0:T(8,128)(2,1)S(1)} all-gather(bf16[2,1,128,128]{3,2,1,0:T(8,128)(2,1)S(1)} %get-tuple-element.354), channel_id=3, replica_groups=mesh['sp'=4,'tp'=8] {'sp'}, dimensions={0}, use_global_device_ids=true | all-gather | bytes 327680 | tf_op jit(solution)/shard_map/all_gather | solution.py:14
  170.0 1.1 while.41
  171.1 0.9 fusion.30
  172.0 8.3 %reduce-scatter.4.cloned.1.call-done = f32[512,2]{1,0:T(8,128)} async-done(((f32[4096,2]{1,0:T(8,128)}), f32[512,2]{1,0:T(8,128)}) %reduce-scatter.4.cloned.1.call-update) | async-done | bytes 4112
  180.3 1.6 copy.60
  (74 shorter events, 9.2 us)
Async XLA Ops:
  7.2 4.6 %copy-start = (bf16[4096,128]{1,0:T(8,128)(2,1)S(1)}, bf16[4096,128]{1,0:T(8,128)(2,1)}, u32[]{:S(2)}) copy-start(bf16[4096,128]{1,0:T(8,128)(2,1)} %param.20) | copy-start | bytes 3145732
  7.2 46.2 %copy-start.3 = (f32[2,256,1]{1,2,0:T(1,128)S(1)}, f32[2,256,1]{1,2,0:T(1,128)}, u32[]{:S(2)}) copy-start(f32[2,256,1]{1,2,0:T(1,128)} %param.27) | copy-start | bytes 6148
  7.2 42.8 %all-gather.5.cloned.1.call-start = ((), (), s32[]{:S(2)}) async-start(), calls=%async_computation.1 | async-start | bytes 4718592 | tf_op jit(solution)/shard_map/all_gather | solution.py:124
  7.9 172.3 %reduce-scatter.4.cloned.1.call-start = ((), (), s32[]{:S(2)}) async-start(), calls=%async_computation.2 | async-start | bytes 2359296
  54.1 44.4 %copy-start.5 = (bf16[4096,128]{1,0:T(8,128)(2,1)S(1)}, bf16[4096,128]{1,0:T(8,128)(2,1)}, u32[]{:S(2)}) copy-start(bf16[4096,128]{1,0:T(8,128)(2,1)} %param.21) | copy-start | bytes 3145732
  106.1 30.8 %copy-start.2 = (bf16[2,4096]{1,0:T(2,128)(2,1)S(1)}, bf16[2,4096]{1,0:T(2,128)(2,1)}, u32[]{:S(2)}) copy-start(bf16[2,4096]{1,0:T(2,128)(2,1)} %param.19) | copy-start | bytes 49156
  106.1 32.4 %copy-start.1 = (bf16[128,4096]{1,0:T(8,128)(2,1)S(1)}, bf16[128,4096]{1,0:T(8,128)(2,1)}, u32[]{:S(2)}) copy-start(bf16[128,4096]{1,0:T(8,128)(2,1)} %param.29) | copy-start | bytes 3145732
  106.1 32.4 %copy-start.4 = (f32[128]{0:T(128)S(1)}, f32[128]{0:T(128)}, u32[]{:S(2)}) copy-start(f32[128]{0:T(128)} %param.28) | copy-start | bytes 1540
Sparse Core Ops, SparseCore 0:
  9.9 40.0 all-gather.4
  141.9 38.3 reduce-scatter.3
where the time goes:
time: 189 us
  blocking collectives  56.6 us (30%)
  waiting for transfers between devices  43.9 us (23%)
  other arithmetic  41.5 us (22%)
  matrix products  26.6 us (14%)
  between operations  15 us (8%)
  local copies, waits for them, and re-layouts  4.71 us (2%)
    another operation x1, other arithmetic, segment_map(): lax.linalg.triangular_solve(system, targets, left_side=True, lower=True)  39.3 us
    all_gather x1, waiting for transfers between devices, body(): portion = lax.all_gather(context_activations, 'tp', axis=2, tiled=True)  34.9 us
    all_gather x2, blocking collectives, carried_in(): lax.all_gather(part.astype(kind), axis)  28.2 us
    all_gather x1, blocking collectives, carried_in_2(): everything = lax.all_gather(value, axis)  16.2 us
    psum x1, blocking collectives, body(): read = lax.psum(term, 'sp') + own_write  12.1 us
    unnamed x3, waiting for transfers between devices  8.97 us
  transfers between devices with their start and end apart: 2, of which 2 were waited for; matrix products, arithmetic and copies ran while one was open for 4% of the time, Pallas kernels for 0%

commit v1 on v0

--- a/solution.py
+++ b/solution.py
@@ -121,7 +121,7 @@
     logit_weight = jnp.concatenate([beta_cols, decay_cols], axis=1)
     fading_speeds = lax.dynamic_slice_in_dim(channel_fading_speed, first_head, current_heads, 0)
     seq_count, length = (context_activations.shape[0], context_activations.shape[1])
-    portion = lax.all_gather(context_activations, "tp", axis=2, tiled=True)
+    portion = jnp.concatenate(lax.all_gather(context_activations, "tp"), axis=2)
     key_sum = jnp.einsum(
         "abf,fc->abc", portion, address_projection, preferred_element_type=jnp.float32
     )

time: 189 us -> 230 us (1.22)
  waiting for transfers between devices: 43.9 us -> 72.6 us
  local copies, waits for them, and re-layouts: 4.71 us -> 18.5 us
    unnamed x3, waiting for transfers between devices: 8.97 us -> 38.3 us
    reshape x0 -> x1, local copies, waits for them, and re-layouts: none -> 7.41 us  [body(): portion = jnp.concatenate(lax.all_gather(context_activations, 'tp'), axis=2)]
    all_gather x0 -> x1, local copies, waits for them, and re-layouts: none -> 6.5 us  [body(): portion = jnp.concatenate(lax.all_gather(context_activations, 'tp'), axis=2)]
  transfers between devices with their start and end apart: 2 -> 2, of which waited for: 2 -> 2; matrix products, arithmetic and copies ran while one was open for 4% -> 3% of each run, Pallas kernels for 0% -> 0%
where the time goes in v1:
time: 230 us; the launch traced here: 229 us
  waiting for transfers between devices  72.6 us (32%)
  blocking collectives  56.7 us (25%)
  other arithmetic  41.3 us (18%)
  matrix products  24.9 us (11%)
  local copies, waits for them, and re-layouts  18.5 us (8%)
  between operations  14.9 us (6%)
    another operation x1, other arithmetic, segment_map(): lax.linalg.triangular_solve(system, targets, left_side=True, lower=True)  39.3 us
    unnamed x3, waiting for transfers between devices  38.3 us
    all_gather x1, waiting for transfers between devices, body(): portion = jnp.concatenate(lax.all_gather(context_activations, 'tp'), axis=2)  34.3 us
    all_gather x2, blocking collectives, carried_in(): lax.all_gather(part.astype(kind), axis)  28.6 us
    all_gather x1, blocking collectives, carried_in_2(): everything = lax.all_gather(value, axis)  16 us
    psum x1, blocking collectives, body(): read = lax.psum(term, 'sp') + own_write  12.1 us
    reshape x1, local copies, waits for them, and re-layouts, body(): portion = jnp.concatenate(lax.all_gather(context_activations, 'tp'), axis=2)  7.41 us
    all_gather x1, local copies, waits for them, and re-layouts, body(): portion = jnp.concatenate(lax.all_gather(context_activations, 'tp'), axis=2)  6.5 us
  transfers between devices with their start and end apart: 2, of which 2 were waited for; matrix products, arithmetic and copies ran while one was open for 3% of the time, Pallas kernels for 0%

profile of v1, /device:TPU:0, one launch (start us, length us, event | category | flops | bytes accessed | tf_op | source)
XLA Modules:
  0.0 229.4 jit_solution(9054388824659149136)
XLA Ops:
  8.0 1.2 dynamic_slice.48
  10.0 1.6 multiply_reduce_fusion.4
  11.6 1.1 multiply_reduce_fusion.3
  12.9 0.9 constant_dynamic-slice_fusion.1
  13.8 0.9 convolution_bitcast_fusion.6
  14.9 34.3 %all-gather.6.cloned.1.call-done = bf16[16,256,512]{2,1,0:T(8,128)(2,1)} async-done(((bf16[2,256,512]{2,1,0:T(8,128)(2,1)}), bf16[16,256,512]{2,1,0:T(8,128)(2,1)}) %all-gather.6.cloned.1.call-update) | async-done | bytes 4194320 | tf_op jit(solution)/shard_map/all_gather | solution.py:124
  49.2 6.5 %copy.70 = bf16[8,2,256,512]{3,0,2,1:T(8,128)(2,1)} copy(bf16[8,2,256,512]{3,2,1,0:T(8,128)(2,1)} %bitcast.219) | data formatting | bytes 8388608 | tf_op jit(solution)/shard_map/all_gather | solution.py:124
  55.7 7.4 %reshape.321 = bf16[2,256,4096]{2,1,0:T(8,128)(2,1)} reshape(bf16[2,256,8,512]{3,2,1,0:T(8,128)(2,1)} %bitcast.218) | data formatting | bytes 8388608 | tf_op jit(solution)/shard_map/reshape | solution.py:124
  63.1 3.5 %fusion.31 = bf16[2,256,2]{1,2,0:T(2,128)(2,1)S(1)} fusion(bf16[2,256,4096]{2,1,0:T(8,128)(2,1)} %reshape.321, bf16[4096,1]{0,1:T(2,128)(2,1)S(1)} %get-tuple-element.365, bf16[4096,1]{0,1:T(2,128)(2,1)S(1)} %get-tuple-element.366), kind=kOutput, calls=%fused_computation.42 | convolution fusion | flops 8422400 | bytes 4212736 | tf_op jit(solution)/shard_map/abf,fc->abc/dot_general | solution.py:131
  66.7 1.4 multiply_reduce_fusion
  69.6 3.8 %multiply_convert_fusion = bf16[2,256,128]{2,1,0:T(8,128)(2,1)S(1)} fusion(bf16[2,256,4096]{2,1,0:T(8,128)(2,1)} %reshape.321, bf16[4096,128]{1,0:T(8,128)(2,1)} %param.21), kind=kOutput, calls=%fused_computation.57 | convolution fusion | flops 537198592 | bytes 5373952 | tf_op jit(solution)/shard_map/abf,fc->abc/dot_general | solution.py:128
  74.0 39.3 %custom-call.3 = f32[2,1,4,1,64,64]{4,5,3,2,1,0:T(8,128)S(1)} custom-call(f32[2,1,4,1,64,64]{5,4,3,2,1,0:T(8,128)S(1)} %fusion.27), custom_call_target="InvertDiagBlocksLowerTriangular" | custom-call | tf_op jit(solution)/shard_map/vmap(vmap())/triangular_solve | solution.py:74
  114.4 3.0 %while.39 = (s32[]{:T(128)}, f32[2,1,128,256]{3,2,0,1:T(8,128)S(1)}, f32[4,2,1]{1,2,0:T(1,128)S(1)}, f32[4,2,1,64,128]{4,3,0,1,2:T(8,128)S(1)}, f32[4,2,1,64,256...) while((s32[]{:T(128)}, f32[2,1,128,256]{3,2,0,1:T(8,128)S(1)}, ...), condition=%wide.region_3.4_spmd, body=%wide.region_2.3_spmd.sunk | while | flops 100827136 | bytes 1312365 | solution.py:94
  117.4 13.9 %all-gather.2 = bf16[8,1,128,128]{3,2,1,0:T(8,128)(2,1)S(1)} all-gather(bf16[2,1,128,128]{3,2,1,0:T(8,128)(2,1)S(1)} %get-tuple-element.354), channel_id=4, replica_groups=mesh['sp'=4,'tp'=8] {'sp'}, dimensions={0}, use_global_device_ids=true | all-gather | bytes 327680 | tf_op jit(solution)/shard_map/all_gather | solution.py:14
  131.4 14.6 %all-gather.1 = bf16[8,1,128,128]{3,2,1,0:T(8,128)(2,1)S(1)} all-gather(bf16[2,1,128,128]{3,2,1,0:T(8,128)(2,1)S(1)} %get-tuple-element.355), channel_id=3, replica_groups=mesh['sp'=4,'tp'=8] {'sp'}, dimensions={0}, use_global_device_ids=true | all-gather | bytes 327680 | tf_op jit(solution)/shard_map/all_gather | solution.py:14
  146.0 1.1 while.41
  147.1 16.0 %all-gather.3 = f32[8,1,128,128]{3,2,1,0:T(8,128)S(1)} all-gather(f32[2,1,128,128]{3,2,1,0:T(8,128)S(1)} %slice_bitcast_fusion.1), channel_id=5, replica_groups=mesh['sp'=4,'tp'=8] {'sp'}, dimensions={0}, use_global_device_ids=true | all-gather | bytes 655360 | tf_op jit(solution)/shard_map/all_gather | solution.py:36
  163.0 1.8 while.40
  165.4 12.1 %psum.7 = f32[2,1,128]{2,0,1:T(2,128)S(1)} all-reduce(f32[2,1,128]{2,0,1:T(2,128)S(1)} %bitcast.230), channel_id=1, replica_groups=mesh['sp'=4,'tp'=8] {'sp'}, use_global_device_ids=true, to_apply=%region_11.12 | all-reduce | flops 256 | bytes 2048 | tf_op jit(solution)/shard_map/psum | solution.py:190
  177.5 1.6 multiply_reduce_fusion.1
  179.1 3.3 %convolution_bitcast_fusion.2 = f32[4096,2]{1,0:T(8,128)} fusion(bf16[128,4096]{1,0:T(8,128)(2,1)S(1)} %copy-done.2, f32[2,1,128]{2,0,1:T(2,128)S(1)} %get-tuple-element.345, f32[128]{0:T(128)S(1)} %copy-done.5, f32[2]{0:T(128)S(1)} %add_rsqrt_fusion.1, bf16[2,4096]{1,0:T(2,128)(2,1)S(1)} %copy-done.3, bf16[4096,128]{1,0:T(8,128)(2,1)} %param.23), kind=kOutput, calls=%fused_computation.29 | convolution fusion | flops 4196352 | bytes 2147848
  182.4 0.9 fusion.30
  183.3 37.6 %reduce-scatter.4.cloned.1.call-done = f32[512,2]{1,0:T(8,128)} async-done(((f32[4096,2]{1,0:T(8,128)}), f32[512,2]{1,0:T(8,128)}) %reduce-scatter.4.cloned.1.call-update) | async-done | bytes 4112
  220.9 1.6 copy.63
  (76 shorter events, 10.5 us)
Async XLA Ops:
  7.2 4.4 %copy-start = (bf16[4096,128]{1,0:T(8,128)(2,1)S(1)}, bf16[4096,128]{1,0:T(8,128)(2,1)}, u32[]{:S(2)}) copy-start(bf16[4096,128]{1,0:T(8,128)(2,1)} %param.20) | copy-start | bytes 3145732
  7.2 42.0 %all-gather.6.cloned.1.call-start = ((), (), s32[]{:S(2)}) async-start(), calls=%async_computation.1 | async-start | bytes 4718592 | tf_op jit(solution)/shard_map/all_gather | solution.py:124
  7.9 213.0 %reduce-scatter.4.cloned.1.call-start = ((), (), s32[]{:S(2)}) async-start(), calls=%async_computation.2 | async-start | bytes 2359296
  63.1 3.5 %copy-start.1 = (bf16[2,256,4096]{2,1,0:T(8,128)(2,1)S(1)}, bf16[2,256,4096]{2,1,0:T(8,128)(2,1)}, u32[]{:S(2)}) copy-start(bf16[2,256,4096]{2,1,0:T(8,128)(2,1)} %reshape.321) | copy-start | bytes 12582916
  66.7 1.4 copy-start.4
  131.3 46.2 %copy-start.3 = (bf16[2,4096]{1,0:T(2,128)(2,1)S(1)}, bf16[2,4096]{1,0:T(2,128)(2,1)}, u32[]{:S(2)}) copy-start(bf16[2,4096]{1,0:T(2,128)(2,1)} %param.19) | copy-start | bytes 49156
  146.0 33.1 %copy-start.2 = (bf16[128,4096]{1,0:T(8,128)(2,1)S(1)}, bf16[128,4096]{1,0:T(8,128)(2,1)}, u32[]{:S(2)}) copy-start(bf16[128,4096]{1,0:T(8,128)(2,1)} %param.29) | copy-start | bytes 3145732
  146.0 33.1 %copy-start.5 = (f32[128]{0:T(128)S(1)}, f32[128]{0:T(128)}, u32[]{:S(2)}) copy-start(f32[128]{0:T(128)} %param.28) | copy-start | bytes 1540
Sparse Core Ops, SparseCore 0:
  9.9 39.2 all-gather.5
  182.6 38.3 reduce-scatter.3
